TPU v7x, 32 devices: a whole 2x2x4 slice. The times are simulated.
32 devices in a mesh: sp: 8 (over z, x), tp: 4 (over y, core).
Axes of the slice: x: 2, y: 2, z: 4, core: 2. Of those that a mesh axis runs over, the one named last changes fastest.
Arguments:
- residual: bfloat16 [2048, 2048], P(('sp', 'tp')), may hold values from -6 to 6
- queries: bfloat16 [2048, 1024], P('sp', 'tp'), may hold values from -8 to 8
- key_pairs: bfloat16 [2048, 512], P('sp', 'tp'), may hold values from -8 to 8
- values: bfloat16 [2048, 512], P('sp', 'tp'), may hold values from -6 to 6
- lambdas: float32 [8], P('tp'), may hold values from 0.3 to 0.8
- head_gain: float32 [128], replicated, may hold values from 0.1 to 1.9
- out_weight: bfloat16 [1024, 2048], replicated, may hold values from -0.1875 to 0.1875
- mixer_gain: float32 [2048], replicated, may hold values from 0.1 to 1.9
- before_gain: float32 [2048], replicated, may hold values from 0.1 to 1.9
- after_gain: float32 [2048], replicated, may hold values from 0.1 to 1.9
- gate_weight: bfloat16 [2048, 5632], P('sp', 'tp'), may hold values from -0.125 to 0.125
- up_weight: bfloat16 [2048, 5632], P('sp', 'tp'), may hold values from -0.125 to 0.125
- down_weight: bfloat16 [5632, 2048], P('tp', 'sp'), may hold values from -0.078125 to 0.078125
Outputs:
- updated: bfloat16 [2048, 2048], P(('sp', 'tp'))
All inputs are finite; a program needn't handle non-finite values.
Results may differ from a plain program's by a relative error of at most 0.014.
Values may be sent and summed in bfloat16 or wider, within the bound.
A program may use at most 128 MiB of HBM per device.

v0:
```python
import math

import jax
import jax.numpy as jnp
from jax import lax
from jax.sharding import PartitionSpec as P

HEAD_DIM = 64


def row_norm(values_in, gain, epsilon):
    mean_square = jnp.mean(values_in * values_in, axis=-1, keepdims=True)
    return values_in * lax.rsqrt(mean_square + epsilon) * gain


def on_device(
    residual,
    queries,
    key_pairs,
    values,
    lambdas,
    head_gain,
    out_weight,
    mixer_gain,
    before_gain,
    after_gain,
    gate_weight,
    up_weight,
    down_weight,
):
    tokens_here = queries.shape[0]
    quarter = residual.shape[0]
    width = 2 * HEAD_DIM
    local_heads = queries.shape[1] // width
    scale = 1.0 / math.sqrt(HEAD_DIM)
    height = local_heads * tokens_here
    query_rows = jnp.transpose(
        queries.reshape(tokens_here, local_heads, 2, HEAD_DIM), (2, 1, 0, 3)
    ).reshape(2, height, HEAD_DIM)
    empty = (
        jnp.full((height,), -1e30, jnp.float32),
        jnp.zeros((height,), jnp.float32),
        jnp.zeros((height, width), jnp.float32),
    )
    state = (empty, empty)
    key_piece = lax.all_gather(key_pairs, "sp", axis=0, tiled=True)
    value_piece = lax.all_gather(values, "sp", axis=0, tiled=True)
    length = key_piece.shape[0]
    span = length
    for split_count in range(1, length + 1):
        if length % split_count == 0 and length // split_count <= 2048:
            span = length // split_count
            break
    key_blocks = key_piece.reshape(length // span, span, 2, HEAD_DIM)
    value_blocks = value_piece.reshape(length // span, span, width)

    def advance(carry, blocks_in):
        key_block, value_block = blocks_in
        renewed = []
        for which in range(2):
            running_top, running_total, running_numer = carry[which]
            score = (
                jnp.dot(
                    query_rows[which], key_block[:, which].T, preferred_element_type=jnp.float32
                )
                * scale
            )
            new_top = jnp.maximum(running_top, jnp.max(score, axis=1))
            shrink = jnp.exp(running_top - new_top)
            expo = jnp.exp(score - new_top[:, None])
            new_total = running_total * shrink + jnp.sum(expo, axis=1)
            new_numer = running_numer * shrink[:, None] + jnp.dot(
                expo.astype(jnp.bfloat16), value_block, preferred_element_type=jnp.float32
            )
            renewed.append((new_top, new_total, new_numer))
        return (tuple(renewed), None)

    state, _ = lax.scan(advance, state, (key_blocks, value_blocks))
    first_map, second_map = state
    lambda_rows = jnp.repeat(lambdas, tokens_here)[:, None]
    attended = first_map[2] / first_map[1][:, None] - lambda_rows * (
        second_map[2] / second_map[1][:, None]
    )
    normed = row_norm(attended, head_gain, 1e-05).astype(jnp.bfloat16)
    head_out = jnp.transpose(normed.reshape(local_heads, tokens_here, width), (1, 0, 2)).reshape(
        tokens_here, local_heads * width
    )
    grouped = head_out.reshape(lax.axis_size("tp"), quarter, local_heads * width)
    mixed = jnp.dot(
        lax.all_to_all(grouped, "tp", split_axis=0, concat_axis=2, tiled=True)[0],
        out_weight,
        preferred_element_type=jnp.float32,
    ).astype(jnp.bfloat16)[None][0]
    stream = residual.astype(jnp.float32) + row_norm(mixed.astype(jnp.float32), mixer_gain, 1e-06)
    normed_in = row_norm(stream, before_gain, 1e-06).astype(jnp.bfloat16)
    gathered = lax.all_gather(normed_in, "tp", axis=0, tiled=True)
    empty_hidden = jnp.zeros((gathered.shape[0], gate_weight.shape[1]), jnp.float32)
    pieces = (
        lax.all_gather(gate_weight, "sp", axis=0, tiled=True),
        lax.all_gather(up_weight, "sp", axis=0, tiled=True),
    )
    columns = lax.slice_in_dim(gathered, 0, pieces[0].shape[0], axis=1)
    gate_part = jnp.dot(columns, pieces[0], preferred_element_type=jnp.float32)
    up_part = jnp.dot(columns, pieces[1], preferred_element_type=jnp.float32)
    gate = empty_hidden + gate_part
    up = empty_hidden + up_part
    down_whole = lax.all_gather(down_weight, "sp", axis=1, tiled=True)
    hidden = (jax.nn.silu(gate) * up).astype(jnp.bfloat16)
    picked = lax.slice_in_dim(hidden, 0, lax.axis_size("tp") * quarter, axis=0)
    channel = lax.psum_scatter(
        jnp.dot(picked, down_whole, preferred_element_type=jnp.float32).astype(jnp.bfloat16),
        "tp",
        scatter_dimension=0,
        tiled=True,
    )
    updated = stream + 0.5 * row_norm(channel.astype(jnp.float32), after_gain, 1e-06)
    return updated.astype(jnp.bfloat16)


def solution(mesh):
    return jax.shard_map(
        on_device,
        mesh=mesh,
        in_specs=(
            P(("sp", "tp"), None),
            P("sp", "tp"),
            P("sp", "tp"),
            P("sp", "tp"),
            P("tp"),
            P(),
            P(),
            P(),
            P(),
            P(),
            P("sp", "tp"),
            P("sp", "tp"),
            P("tp", "sp"),
        ),
        out_specs=P(("sp", "tp"), None),
        check_vma=False,
    )
```

profile of v0, /device:TPU:1, one launch (start us, length us, event | category | flops | bytes accessed | tf_op | source)
XLA Modules:
  0.0 429.3 jit_solution(3633528644462433819)
XLA Ops:
  6.5 0.0 copy-start
  6.5 0.0 all-gather.5.cloned.1.call-start
  6.5 0.9 copy.16
  7.5 26.9 %all_gather.18 = bf16[2048,128]{0,1:T(8,128)(2,1)S(1)} all-gather(bf16[256,128]{0,1:T(8,128)(2,1)S(1)} %copy.16), channel_id=1, replica_groups=mesh['sp'=8,'tp'=4] {'sp'}, dimensions={0}, use_global_device_ids=true | all-gather | bytes 589824 | tf_op jit(solution)/shard_map/all_gather | solution.py:46
  34.4 1.0 copy.14
  35.5 0.1 copy.15
  35.6 0.0 copy-start.3
  35.6 0.8 multiply_reduce_fusion.1
  36.4 0.8 fusion
  37.2 0.0 copy-done.3
  37.2 25.4 %all_gather.19 = bf16[2048,128]{1,0:T(8,128)(2,1)S(1)} all-gather(bf16[256,128]{1,0:T(8,128)(2,1)S(1)} %copy-done.3), channel_id=1, replica_groups=mesh['sp'=8,'tp'=4] {'sp'}, dimensions={0}, use_global_device_ids=true | all-gather | bytes 589824 | tf_op jit(solution)/shard_map/all_gather | solution.py:47
  62.6 0.1 copy.17
  62.7 0.8 multiply_reduce_fusion
  63.5 0.8 fusion.2
  64.3 0.0 copy-done
  64.3 0.1 broadcast_bitcast_fusion
  64.4 0.9 fusion.29
  65.3 0.0 copy-start.6
  65.3 1.5 multiply_reduce_fusion.4
  66.8 0.0 copy-start.1
  66.8 0.0 copy-start.2
  66.8 0.0 copy-start.4
  66.9 0.0 copy-done.6
  66.9 0.1 multiply_convert_fusion.1
  67.0 0.1 copy.25
  67.2 0.1 reshape_reshape.3
  67.3 18.2 %all_to_all.15 = bf16[4,64,256]{2,1,0:T(8,128)(2,1)S(1)} all-to-all(bf16[4,64,256]{2,1,0:T(8,128)(2,1)S(1)} %reshape_reshape.3), channel_id=1, replica_groups=mesh['sp'=8,'tp'=4] {'tp'}, dimensions={0} | all-to-all | bytes 262144 | tf_op jit(solution)/shard_map/all_to_all | solution.py:90
  85.5 0.1 copy.19
  85.6 3.1 multiply_reduce_fusion.3
  88.7 0.0 copy-done.1
  88.8 0.0 copy-done.2
  88.8 0.3 multiply_reduce_fusion.2
  89.1 0.0 copy-done.4
  89.1 0.9 multiply_convert_fusion
  90.0 0.0 all-gather.5.cloned.1.call-update
  90.0 0.0 all-gather.7.cloned.1.call-start
  90.0 0.7 all-gather.7.cloned.1.call-update
  90.7 0.0 all-gather.11.cloned.1.call-start
  90.8 0.7 all-gather.11.cloned.1.call-update
  91.5 0.0 all-gather.9.cloned.1.call-start
  91.5 0.5 all-gather.9.cloned.1.call-update
  92.0 0.0 reduce-scatter.2.cloned.1.call-start
  92.1 15.8 %all-gather.5.cloned.1.call-done = bf16[256,2048]{1,0:T(8,128)(2,1)} async-done(((bf16[64,2048]{1,0:T(8,128)(2,1)}), bf16[256,2048]{1,0:T(8,128)(2,1)}) %all-gather.5.cloned.1.call-update) | async-done | bytes 1048592 | tf_op jit(solution)/shard_map/all_gather | solution.py:96
  107.8 0.0 copy-start.7
  107.8 92.6 %all-gather.7.cloned.1.call-done = bf16[2048,1408]{1,0:T(8,128)(2,1)} async-done(((bf16[256,1408]{1,0:T(8,128)(2,1)}), bf16[2048,1408]{1,0:T(8,128)(2,1)}) %all-gather.7.cloned.1.call-update) | async-done | bytes 5767184 | tf_op jit(solution)/shard_map/all_gather | solution.py:99
  200.5 4.8 %fusion.45 = f32[256,1408]{1,0:T(8,128)S(1)} fusion(bf16[256,2048]{1,0:T(8,128)(2,1)} %all-gather.5.cloned.1.call-done, bf16[2048,1408]{1,0:T(8,128)(2,1)} %all-gather.7.cloned.1.call-done), kind=kOutput, calls=%fused_computation.58 | convolution fusion | flops 1476395008 | bytes 8257536 | tf_op jit(solution)/shard_map/dot_general | solution.py:103
  205.2 0.0 copy-start.5
  205.2 89.4 %all-gather.11.cloned.1.call-done = bf16[1408,2048]{1,0:T(8,128)(2,1)} async-done(((bf16[1408,256]{1,0:T(8,128)(2,1)}), bf16[1408,2048]{1,0:T(8,128)(2,1)}) %all-gather.11.cloned.1.call-update) | async-done | bytes 5767184 | tf_op jit(solution)/shard_map/all_gather | solution.py:107
  294.6 91.8 %all-gather.9.cloned.1.call-done = bf16[2048,1408]{1,0:T(8,128)(2,1)} async-done(((bf16[256,1408]{1,0:T(8,128)(2,1)}), bf16[2048,1408]{1,0:T(8,128)(2,1)}) %all-gather.9.cloned.1.call-update) | async-done | bytes 5767184 | tf_op jit(solution)/shard_map/all_gather | solution.py:100
  386.4 0.0 copy-done.7
  386.4 8.9 %convolution_convert_fusion = bf16[256,2048]{1,0:T(8,128)(2,1)} fusion(bf16[1408,2048]{1,0:T(8,128)(2,1)} %all-gather.11.cloned.1.call-done, bf16[256,2048]{1,0:T(8,128)(2,1)S(1)} %copy-done.7, bf16[2048,1408]{1,0:T(8,128)(2,1)} %all-gather.9.cloned.1.call-done, f32[256,1408]{1,0:T(8,128)S(1)} %fusion.45), kind=kOutput, calls=%fused_computation.10 | convolution fusion | flops 2955476992 | bytes 15073280 | tf_op jit(solution)/shard_map/dot_general | solution.py:111
  395.3 0.0 reduce-scatter.2.cloned.1.call-update
  395.3 24.5 %reduce-scatter.2.cloned.1.call-done = bf16[64,2048]{1,0:T(8,128)(2,1)} async-done(((bf16[256,2048]{1,0:T(8,128)(2,1)}), bf16[64,2048]{1,0:T(8,128)(2,1)}) %reduce-scatter.2.cloned.1.call-update) | async-done | bytes 262160 | tf_op jit(solution)/shard_map/reduce_scatter | solution.py:110
  419.8 1.1 fusion.32
  420.9 0.0 copy-done.5
  420.9 1.9 fusion.36
  (13 shorter events, 0.1 us)
Async XLA Ops:
  6.5 57.8 %copy-start = (f32[2]{0:T(128)S(1)}, f32[2]{0:T(128)}, u32[]{:S(2)}) copy-start(f32[2]{0:T(128)} %param.17) | copy-start | bytes 28
  6.5 101.3 %all-gather.5.cloned.1.call-start = ((), (), s32[]{:S(2)}) async-start(), calls=%async_computation.2 | async-start | bytes 1310720 | tf_op jit(solution)/shard_map/all_gather | solution.py:96
  35.6 1.7 copy-start.3
  65.3 1.6 copy-start.6
  66.8 21.9 %copy-start.1 = (bf16[64,2048]{1,0:T(8,128)(2,1)S(1)}, bf16[64,2048]{1,0:T(8,128)(2,1)}, u32[]{:S(2)}) copy-start(bf16[64,2048]{1,0:T(8,128)(2,1)} %param.13) | copy-start | bytes 786436
  66.8 21.9 %copy-start.2 = (f32[2048]{0:T(1024)S(1)}, f32[2048]{0:T(1024)}, u32[]{:S(2)}) copy-start(f32[2048]{0:T(1024)} %param.20) | copy-start | bytes 24580
  66.8 22.2 %copy-start.4 = (f32[2048]{0:T(1024)S(1)}, f32[2048]{0:T(1024)}, u32[]{:S(2)}) copy-start(f32[2048]{0:T(1024)} %param.21) | copy-start | bytes 24580
  90.0 110.5 %all-gather.7.cloned.1.call-start = ((), (), s32[]{:S(2)}) async-start(), calls=%async_computation.3 | async-start | bytes 6488064 | tf_op jit(solution)/shard_map/all_gather | solution.py:99
  90.7 203.9 %all-gather.11.cloned.1.call-start = ((), (), s32[]{:S(2)}) async-start(), calls=%async_computation.5 | async-start | bytes 6488064 | tf_op jit(solution)/shard_map/all_gather | solution.py:107
  91.5 294.9 %all-gather.9.cloned.1.call-start = ((), (), s32[]{:S(2)}) async-start(), calls=%async_computation.4 | async-start | bytes 6488064 | tf_op jit(solution)/shard_map/all_gather | solution.py:100
  92.0 327.8 %reduce-scatter.2.cloned.1.call-start = ((), (), s32[]{:S(2)}) async-start(), calls=%async_computation.6 | async-start | bytes 1310720 | tf_op jit(solution)/shard_map/reduce_scatter | solution.py:110
  107.8 278.6 %copy-start.7 = (bf16[256,2048]{1,0:T(8,128)(2,1)S(1)}, bf16[256,2048]{1,0:T(8,128)(2,1)}, u32[]{:S(2)}) copy-start(bf16[256,2048]{1,0:T(8,128)(2,1)} %all-gather.5.cloned.1.call-done) | copy-start | bytes 3145732
  205.2 215.7 %copy-start.5 = (f32[2048]{0:T(1024)S(1)}, f32[2048]{0:T(1024)}, u32[]{:S(2)}) copy-start(f32[2048]{0:T(1024)} %param.22) | copy-start | bytes 24580
Sparse Core Ops, SparseCore 0:
  90.1 17.7 all-gather.4
  110.0 90.3 all-gather.6
  202.5 92.0 all-gather.10
  296.6 89.7 all-gather.8
  395.4 24.3 reduce-scatter.1
where the time goes:
time: 431 us; the launch traced here: 429 us
  waiting for transfers between devices  316 us (73%)
  blocking collectives  70.5 us (16%)
  matrix products  20.8 us (5%)
  between operations  13.4 us (3%)
  other arithmetic  6 us (1%)
    all_gather x1, waiting for transfers between devices, on_device(): lax.all_gather(gate_weight, 'sp', axis=0, tiled=True)  92.6 us
    all_gather x1, waiting for transfers between devices, on_device(): lax.all_gather(up_weight, 'sp', axis=0, tiled=True)  91.8 us
    all_gather x1, waiting for transfers between devices, on_device(): down_whole = lax.all_gather(down_weight, 'sp', axis=1, tiled=True)  89.4 us
    all_gather x1, blocking collectives, on_device(): key_piece = lax.all_gather(key_pairs, 'sp', axis=0, tiled=True)  26.9 us
    all_gather x1, blocking collectives, on_device(): value_piece = lax.all_gather(values, 'sp', axis=0, tiled=True)  25.4 us
    reduce_scatter x1, waiting for transfers between devices, on_device(): lax.psum_scatter(jnp.dot(picked, down_whole, preferred_element_type=jnp.f...  24.5 us
    all_to_all x1, blocking collectives, on_device(): lax.all_to_all(grouped, 'tp', split_axis=0, concat_axis=2, tiled=True)[0]  18.2 us
    all_gather x1, waiting for transfers between devices, on_device(): gathered = lax.all_gather(normed_in, 'tp', axis=0, tiled=True)  15.8 us
  transfers between devices with their start and end apart: 5, of which 5 were waited for; matrix products, arithmetic and copies ran while one was open for 1% of the time, Pallas kernels for 0%

commit v1 on v0

--- a/solution.py
+++ b/solution.py
@@ -3,6 +3,8 @@
 import jax
 import jax.numpy as jnp
 from jax import lax
+from jax.experimental import pallas as pl
+from jax.experimental.pallas import tpu as pltpu
 from jax.sharding import PartitionSpec as P
 
 HEAD_DIM = 64
@@ -117,9 +119,316 @@
     return updated.astype(jnp.bfloat16)
 
 
+MESH = pl.DeviceIdType.MESH
+
+
+def flip(index, bits):
+    bit = 1
+    while bit <= bits:
+        if bits & bit:
+            index = index + bit - 2 * bit * ((index // bit) % 2)
+        bit *= 2
+    return index
+
+
+def layer(
+    residual,
+    queries,
+    pair,
+    lambdas,
+    head_gain,
+    out_weight,
+    mixer_gain,
+    before_gain,
+    after_gain,
+    gate_in,
+    up_in,
+    down_in,
+    updated,
+    kv,
+    gate_w,
+    up_w,
+    down_w,
+    head_out,
+    head_in,
+    stream,
+    x,
+    p,
+    from_core,
+    from_y,
+    from_z,
+    send_sems,
+    recv_sems,
+    local_sems,
+):
+    depth = gate_in.shape[0]
+    n_tp = head_in.shape[0]
+    quarter, width_all = residual.shape
+    width = 2 * HEAD_DIM
+    heads = queries.shape[1] // width
+    place, member = lax.axis_index("sp"), lax.axis_index("tp")
+    used = [0]
+    copies = []
+
+    def send(src, dst, axis, bits):
+        at = used[0]
+        used[0] += 1
+        target = flip(place if axis == "sp" else member, bits)
+        copy = pltpu.make_async_remote_copy(
+            src_ref=src,
+            dst_ref=dst,
+            send_sem=send_sems.at[at],
+            recv_sem=recv_sems.at[at],
+            device_id={axis: target},
+            device_id_type=MESH,
+        )
+        copy.start()
+        copies.append(copy)
+        return copy
+
+    partners = [("sp", 1)] + [("sp", 2 * j) for j in range(1, depth)]
+    partners += [("tp", j) for j in range(1, n_tp)]
+    barrier = pltpu.get_barrier_semaphore()
+    for axis, bits in partners:
+        target = flip(place if axis == "sp" else member, bits)
+        pl.semaphore_signal(barrier, inc=1, device_id={axis: target}, device_id_type=MESH)
+    pl.semaphore_wait(barrier, len(partners))
+
+    kv_z = [send(pair, kv.at[j], "sp", 2 * j) for j in range(1, depth)]
+    kv_x = [send(pair, kv.at[depth], "sp", 1)]
+
+    def scatter(source, target, at):
+        mine = source.at[place // 2]
+        local = pltpu.make_async_copy(mine, target.at[place], local_sems.at[at])
+        local.start()
+        over_z = [
+            send(source.at[flip(place, 2 * j) // 2], target.at[place], "sp", 2 * j)
+            for j in range(1, depth)
+        ]
+        return local, over_z, send(mine, target.at[place], "sp", 1)
+
+    def forward(target, over_z):
+        over_x = []
+        for j in range(1, depth):
+            over_z[j - 1].wait_recv()
+            slot = target.at[flip(place, 2 * j)]
+            over_x.append(send(slot, slot, "sp", 1))
+        return over_x
+
+    gate_moves = scatter(gate_in, gate_w, 0)
+    up_moves = scatter(up_in, up_w, 1)
+    kv[0] = pair[...]
+    for j in range(1, depth):
+        kv_z[j - 1].wait_recv()
+        kv_x.append(send(kv.at[j], kv.at[depth + j], "sp", 1))
+    for copy in kv_x:
+        copy.wait_recv()
+
+    def attend(tile, _):
+        rows = pl.ds(pl.multiple_of(tile * quarter, quarter), quarter)
+        for h in range(heads):
+            parts = []
+            for which in range(2):
+                start = (2 * h + which) * HEAD_DIM
+                query = queries[rows, start : start + HEAD_DIM]
+                keys = kv[:, :, which * HEAD_DIM : (which + 1) * HEAD_DIM]
+                keys = keys.reshape(2 * depth * keys.shape[1], HEAD_DIM)
+                score = lax.dot_general(
+                    query, keys, (((1,), (1,)), ((), ())), preferred_element_type=jnp.float32
+                ) * (1.0 / math.sqrt(HEAD_DIM))
+                expo = jnp.exp(score - jnp.max(score, axis=1, keepdims=True))
+                total = jnp.sum(expo, axis=1, keepdims=True)
+                vals = kv[:, :, width : 2 * width]
+                vals = vals.reshape(2 * depth * vals.shape[1], width)
+                numer = jnp.dot(
+                    expo.astype(jnp.bfloat16), vals, preferred_element_type=jnp.float32
+                )
+                parts.append(numer / total)
+            attended = parts[0] - lambdas[h] * parts[1]
+            normed = row_norm(attended, head_gain[...], 1e-05).astype(jnp.bfloat16)
+            head_out[tile, :, h * width : (h + 1) * width] = normed
+        return 0
+
+    lax.fori_loop(0, n_tp, attend, 0)
+    moved = [send(head_out.at[flip(member, j)], head_in.at[member], "tp", j) for j in range(1, n_tp)]
+    head_in[member] = head_out[member]
+    gate_x = forward(gate_w, gate_moves[1])
+    for copy in moved:
+        copy.wait_recv()
+    step = head_in.shape[2]
+    mixed = jnp.zeros((quarter, width_all), jnp.float32)
+    for m in range(n_tp):
+        mixed = mixed + jnp.dot(
+            head_in[m], out_weight[m * step : (m + 1) * step], preferred_element_type=jnp.float32
+        )
+    mixed = mixed.astype(jnp.bfloat16).astype(jnp.float32)
+    stream[...] = residual[...].astype(jnp.float32) + row_norm(mixed, mixer_gain[...], 1e-06)
+    x[0] = row_norm(stream[...], before_gain[...], 1e-06).astype(jnp.bfloat16)
+
+    half = 2 * depth
+    x_c = [send(x.at[0], x.at[half], "tp", 1)]
+    x_z = [send(x.at[0], x.at[j], "sp", 2 * j) for j in range(1, depth)]
+    x_y = [send(x.at[0], x.at[depth], "tp", 2)]
+    down_moves = scatter(down_in, down_w, 2)
+    up_x = forward(up_w, up_moves[1])
+    for j in range(1, depth):
+        x_z[j - 1].wait_recv()
+        x_y.append(send(x.at[j], x.at[depth + j], "tp", 2))
+        x_c.append(send(x.at[j], x.at[half + j], "tp", 1))
+    x_last = []
+    for j in range(depth):
+        x_y[j].wait_recv()
+        x_last.append(send(x.at[depth + j], x.at[half + depth + j], "tp", 1))
+    down_x = forward(down_w, down_moves[1])
+
+    for local, _, over_x in (gate_moves, up_moves, down_moves):
+        local.wait()
+        over_x.wait_recv()
+    for copy in gate_x + up_x + down_x:
+        copy.wait_recv()
+
+    blocks = gate_w.shape[0]
+    units = gate_w.shape[2]
+    span = down_w.shape[2]
+
+    def mix(tile, _):
+        rows = x[pl.ds(2 * tile, 2)].reshape(2 * quarter, width_all)
+        gate = jnp.dot(
+            rows, gate_w[...].reshape(width_all, units), preferred_element_type=jnp.float32
+        )
+        up = jnp.dot(rows, up_w[...].reshape(width_all, units), preferred_element_type=jnp.float32)
+        hidden = (gate / (1.0 + jnp.exp(-gate)) * up).astype(jnp.bfloat16)
+        for m in range(blocks):
+            part = jnp.dot(hidden, down_w[m], preferred_element_type=jnp.float32)
+            p[pl.ds(2 * tile, 2), :, m * span : (m + 1) * span] = part.astype(
+                jnp.bfloat16
+            ).reshape(2, quarter, span)
+        return 0
+
+    def group(at):
+        lax.fori_loop(at * depth // 2, (at + 1) * depth // 2, mix, 0)
+
+    group(0)
+    for copy in x_c:
+        copy.wait_recv()
+    group(2)
+    r_c = [send(p.at[half + j], from_core.at[j], "tp", 1) for j in range(depth)]
+    for copy in x_last:
+        copy.wait_recv()
+    group(3)
+    r_d = [send(p.at[half + depth + j], from_core.at[depth + j], "tp", 1) for j in range(depth)]
+    group(1)
+    r_y = []
+    order = list(range(1, depth)) + [0]
+    for j in order:
+        r_d[j].wait_recv()
+        p[depth + j] = (
+            p[depth + j].astype(jnp.float32) + from_core[depth + j].astype(jnp.float32)
+        ).astype(jnp.bfloat16)
+        r_y.append(send(p.at[depth + j], from_y.at[j], "tp", 2))
+    r_z = []
+    for i, j in enumerate(order):
+        r_c[j].wait_recv()
+        r_y[i].wait_recv()
+        total = (
+            p[j].astype(jnp.float32)
+            + from_core[j].astype(jnp.float32)
+            + from_y[j].astype(jnp.float32)
+        )
+        if j:
+            p[j] = total.astype(jnp.bfloat16)
+            r_z.append(send(p.at[j], from_z.at[j - 1], "sp", 2 * j))
+    for j in range(1, depth):
+        r_z[j - 1].wait_recv()
+        total = total + from_z[j - 1].astype(jnp.float32)
+    channel = total.astype(jnp.bfloat16).astype(jnp.float32)
+    updated[...] = (stream[...] + 0.5 * row_norm(channel, after_gain[...], 1e-06)).astype(
+        updated.dtype
+    )
+    for copy in copies:
+        copy.wait_send()
+
+
+def one_kernel(
+    residual,
+    queries,
+    key_pairs,
+    values,
+    lambdas,
+    head_gain,
+    out_weight,
+    mixer_gain,
+    before_gain,
+    after_gain,
+    gate_weight,
+    up_weight,
+    down_weight,
+):
+    n_sp, n_tp = lax.axis_size("sp"), lax.axis_size("tp")
+    depth = n_sp // 2
+    quarter, width_all = residual.shape
+    tokens_here, query_width = queries.shape
+    inner, units_all = gate_weight.shape
+    units = units_all // depth
+    span = down_weight.shape[1]
+    pair = jnp.concatenate([key_pairs, values], axis=1)
+    gate_in = jnp.transpose(gate_weight.reshape(inner, depth, units), (1, 0, 2))
+    up_in = jnp.transpose(up_weight.reshape(inner, depth, units), (1, 0, 2))
+    down_in = down_weight.reshape(depth, units, span)
+    tiles = 4 * depth
+    total_sends = 7 * (depth - 1) + 4 + 3 + 3 * depth - 3 + n_tp - 1 + 2 * tiles
+    vmem = pl.BlockSpec(memory_space=pltpu.VMEM)
+    hbm = pl.BlockSpec(memory_space=pl.ANY)
+    smem = pl.BlockSpec(memory_space=pltpu.SMEM)
+    bf16 = jnp.bfloat16
+    return pl.pallas_call(
+        layer,
+        out_shape=jax.ShapeDtypeStruct(residual.shape, bf16),
+        in_specs=[vmem, vmem, vmem, smem] + [vmem] * 5 + [hbm] * 3,
+        out_specs=vmem,
+        scratch_shapes=[
+            pltpu.VMEM((n_sp,) + pair.shape, bf16),
+            pltpu.VMEM((n_sp, inner, units), bf16),
+            pltpu.VMEM((n_sp, inner, units), bf16),
+            pltpu.VMEM((n_sp, units, span), bf16),
+            pltpu.VMEM((n_tp, quarter, query_width), bf16),
+            pltpu.VMEM((n_tp, quarter, query_width), bf16),
+            pltpu.VMEM((quarter, width_all), jnp.float32),
+            pltpu.VMEM((tiles, quarter, width_all), bf16),
+            pltpu.VMEM((tiles, quarter, width_all), bf16),
+            pltpu.VMEM((2 * depth, quarter, width_all), bf16),
+            pltpu.VMEM((depth, quarter, width_all), bf16),
+            pltpu.VMEM((depth - 1, quarter, width_all), bf16),
+            pltpu.SemaphoreType.DMA((total_sends,)),
+            pltpu.SemaphoreType.DMA((total_sends,)),
+            pltpu.SemaphoreType.DMA((3,)),
+        ],
+        compiler_params=pltpu.CompilerParams(
+            collective_id=0, has_side_effects=True, vmem_limit_bytes=60 * 1024 * 1024
+        ),
+    )(
+        residual,
+        queries,
+        pair,
+        lambdas,
+        head_gain[None],
+        out_weight,
+        mixer_gain[None],
+        before_gain[None],
+        after_gain[None],
+        gate_in,
+        up_in,
+        down_in,
+    )
+
+
+def fits(mesh):
+    return mesh.shape["tp"] == 4 and mesh.shape["sp"] == 8
+
+
 def solution(mesh):
     return jax.shard_map(
-        on_device,
+        one_kernel if fits(mesh) else on_device,
         mesh=mesh,
         in_specs=(
             P(("sp", "tp"), None),

time: 431 us -> 156 us (0.36)
  the two profiles are of different devices: /device:TPU:1 before, /device:TPU:16 now
where the time goes in v1:
time: 156 us
  Pallas kernels  148 us (95%)
  local copies, waits for them, and re-layouts  6.79 us (4%)
    pallas_call x1, Pallas kernels, one_kernel(): pl.pallas_call(layer, out_shape=jax.ShapeDtypeStruct(residual.shape, bf16...  148 us
    unnamed x7, local copies, waits for them, and re-layouts  4.47 us

profile of v1, /device:TPU:16, one launch (start us, length us, event | category | flops | bytes accessed | tf_op | source)
XLA Modules:
  0.0 155.8 jit_solution(8486505349006365135)
XLA Ops:
  0.0 0.0 copy-start.1
  0.0 0.0 copy-start
  0.0 1.4 copy.14
  1.4 1.2 copy.15
  2.6 1.4 copy.16
  4.0 1.2 copy.17
  5.1 0.0 copy-done.1
  5.1 0.0 copy-done
  5.1 0.7 pad_maximum_fusion.pair
  5.8 148.3 %shard_map.127 = bf16[64,2048]{1,0:T(8,128)(2,1)} custom-call(bf16[64,2048]{1,0:T(8,128)(2,1)} %residual.1, bf16[256,256]{1,0:T(8,128)(2,1)} %queries.1, bf16[256,256]{1,0:T(8,128)(2,1)} %pad_maximum_fusion.pair, f32[2]{0:T(128)} %lambdas.1, f32[1,128]{1,0:T(1,128)} %bitcast.17, bf16[1024,2048]{1,0:T(8,128)(2,1)} %out_weight.1, f32[1,2048]{1,0:T(1,128)} %bitcast.14, ...), custom_call_target="tpu_custom_call" | custom-call | tf_op jit(solution)/shard_map/pallas_call | solution.py:384
  154.1 1.7 %copy.19 = bf16[64,2048]{1,0:T(8,128)(2,1)} copy(bf16[64,2048]{1,0:T(8,128)(2,1)} %shard_map.127) | data formatting | bytes 524288
Async XLA Ops:
  0.0 5.1 %copy-start.1 = (bf16[256,128]{1,0:T(8,128)(2,1)S(1)}, bf16[256,128]{1,0:T(8,128)(2,1)}, u32[]{:S(2)}) copy-start(bf16[256,128]{1,0:T(8,128)(2,1)} %param.15) | copy-start | bytes 196612
  0.0 5.1 %copy-start = (bf16[256,128]{1,0:T(8,128)(2,1)S(1)}, bf16[256,128]{1,0:T(8,128)(2,1)}, u32[]{:S(2)}) copy-start(bf16[256,128]{1,0:T(8,128)(2,1)} %param.16) | copy-start | bytes 196612

commit v2 on v1

--- a/solution.py
+++ b/solution.py
@@ -134,17 +134,21 @@
 def layer(
     residual,
     queries,
-    pair,
+    key_pairs,
+    values,
     lambdas,
     head_gain,
     out_weight,
     mixer_gain,
     before_gain,
     after_gain,
+    gate_weight,
+    up_weight,
+    down_in,
+    updated,
     gate_in,
     up_in,
-    down_in,
-    updated,
+    hidden,
     kv,
     gate_w,
     up_w,
@@ -161,7 +165,7 @@
     recv_sems,
     local_sems,
 ):
-    depth = gate_in.shape[0]
+    depth = down_in.shape[0]
     n_tp = head_in.shape[0]
     quarter, width_all = residual.shape
     width = 2 * HEAD_DIM
@@ -194,8 +198,18 @@
         pl.semaphore_signal(barrier, inc=1, device_id={axis: target}, device_id_type=MESH)
     pl.semaphore_wait(barrier, len(partners))
 
-    kv_z = [send(pair, kv.at[j], "sp", 2 * j) for j in range(1, depth)]
-    kv_x = [send(pair, kv.at[depth], "sp", 1)]
+    kv[0, :, :width] = key_pairs[...]
+    kv[0, :, width:] = values[...]
+    far = send(kv.at[0], kv.at[2], "sp", 4)
+    near = send(kv.at[0], kv.at[1], "sp", 2)
+    kv_x = [send(kv.at[0], kv.at[depth], "sp", 1)]
+    for source, target in ((gate_weight, gate_in), (up_weight, up_in)):
+        columns = target.shape[2]
+        for j in range(depth):
+            target[j] = source[:, j * columns : (j + 1) * columns]
+    far.wait_recv()
+    relayed = send(kv.at[2], kv.at[3], "sp", 2)
+    kv_x.append(send(kv.at[2], kv.at[depth + 2], "sp", 1))
 
     def scatter(source, target, at):
         mine = source.at[place // 2]
@@ -217,9 +231,8 @@
 
     gate_moves = scatter(gate_in, gate_w, 0)
     up_moves = scatter(up_in, up_w, 1)
-    kv[0] = pair[...]
-    for j in range(1, depth):
-        kv_z[j - 1].wait_recv()
+    for j, copy in ((1, near), (3, relayed)):
+        copy.wait_recv()
         kv_x.append(send(kv.at[j], kv.at[depth + j], "sp", 1))
     for copy in kv_x:
         copy.wait_recv()
@@ -266,81 +279,99 @@
     x[0] = row_norm(stream[...], before_gain[...], 1e-06).astype(jnp.bfloat16)
 
     half = 2 * depth
+    far = send(x.at[0], x.at[2], "sp", 4)
+    near = send(x.at[0], x.at[1], "sp", 2)
     x_c = [send(x.at[0], x.at[half], "tp", 1)]
-    x_z = [send(x.at[0], x.at[j], "sp", 2 * j) for j in range(1, depth)]
     x_y = [send(x.at[0], x.at[depth], "tp", 2)]
+    up_x = forward(up_w, up_moves[1])
+    far.wait_recv()
+    relayed = send(x.at[2], x.at[3], "sp", 2)
     down_moves = scatter(down_in, down_w, 2)
-    up_x = forward(up_w, up_moves[1])
-    for j in range(1, depth):
-        x_z[j - 1].wait_recv()
+    order = ((2, far), (1, near), (3, relayed))
+    for j, copy in order:
+        if j != 2:
+            copy.wait_recv()
         x_y.append(send(x.at[j], x.at[depth + j], "tp", 2))
         x_c.append(send(x.at[j], x.at[half + j], "tp", 1))
-    x_last = []
-    for j in range(depth):
-        x_y[j].wait_recv()
-        x_last.append(send(x.at[depth + j], x.at[half + depth + j], "tp", 1))
-    down_x = forward(down_w, down_moves[1])
-
-    for local, _, over_x in (gate_moves, up_moves, down_moves):
+    for local, _, over_x in (gate_moves, up_moves):
         local.wait()
         over_x.wait_recv()
-    for copy in gate_x + up_x + down_x:
+    for copy in gate_x + up_x:
         copy.wait_recv()
 
     blocks = gate_w.shape[0]
     units = gate_w.shape[2]
     span = down_w.shape[2]
 
-    def mix(tile, _):
+    def widen(tile, _):
         rows = x[pl.ds(2 * tile, 2)].reshape(2 * quarter, width_all)
         gate = jnp.dot(
             rows, gate_w[...].reshape(width_all, units), preferred_element_type=jnp.float32
         )
         up = jnp.dot(rows, up_w[...].reshape(width_all, units), preferred_element_type=jnp.float32)
-        hidden = (gate / (1.0 + jnp.exp(-gate)) * up).astype(jnp.bfloat16)
+        hidden[tile] = (gate / (1.0 + jnp.exp(-gate)) * up).astype(jnp.bfloat16)
+        return 0
+
+    def narrow(tile, _):
         for m in range(blocks):
-            part = jnp.dot(hidden, down_w[m], preferred_element_type=jnp.float32)
+            part = jnp.dot(hidden[tile], down_w[m], preferred_element_type=jnp.float32)
             p[pl.ds(2 * tile, 2), :, m * span : (m + 1) * span] = part.astype(
                 jnp.bfloat16
             ).reshape(2, quarter, span)
         return 0
 
-    def group(at):
-        lax.fori_loop(at * depth // 2, (at + 1) * depth // 2, mix, 0)
-
-    group(0)
+    def group(at, body):
+        lax.fori_loop(at * depth // 2, (at + 1) * depth // 2, body, 0)
+
+    group(0, widen)
+    x_last = []
+    for j, copy in zip((0, 2, 1, 3), x_y):
+        copy.wait_recv()
+        x_last.append(send(x.at[depth + j], x.at[half + depth + j], "tp", 1))
+    down_x = forward(down_w, down_moves[1])
     for copy in x_c:
         copy.wait_recv()
-    group(2)
-    r_c = [send(p.at[half + j], from_core.at[j], "tp", 1) for j in range(depth)]
+    group(2, widen)
+    group(1, widen)
     for copy in x_last:
         copy.wait_recv()
-    group(3)
+    group(3, widen)
+    down_moves[0].wait()
+    down_moves[2].wait_recv()
+    for copy in down_x:
+        copy.wait_recv()
+    group(3, narrow)
     r_d = [send(p.at[half + depth + j], from_core.at[depth + j], "tp", 1) for j in range(depth)]
-    group(1)
+    group(1, narrow)
     r_y = []
-    order = list(range(1, depth)) + [0]
-    for j in order:
+    turns = (3, 1, 2, 0)
+    for j in turns:
         r_d[j].wait_recv()
         p[depth + j] = (
             p[depth + j].astype(jnp.float32) + from_core[depth + j].astype(jnp.float32)
         ).astype(jnp.bfloat16)
         r_y.append(send(p.at[depth + j], from_y.at[j], "tp", 2))
+    group(2, narrow)
+    r_c = [send(p.at[half + j], from_core.at[j], "tp", 1) for j in range(depth)]
+    group(0, narrow)
     r_z = []
-    for i, j in enumerate(order):
+    for copy, j in zip(r_y, turns):
         r_c[j].wait_recv()
-        r_y[i].wait_recv()
+        copy.wait_recv()
         total = (
             p[j].astype(jnp.float32)
             + from_core[j].astype(jnp.float32)
             + from_y[j].astype(jnp.float32)
         )
+        if j == 2:
+            r_z[0].wait_recv()
+            total = total + from_z[2].astype(jnp.float32)
         if j:
             p[j] = total.astype(jnp.bfloat16)
-            r_z.append(send(p.at[j], from_z.at[j - 1], "sp", 2 * j))
-    for j in range(1, depth):
-        r_z[j - 1].wait_recv()
-        total = total + from_z[j - 1].astype(jnp.float32)
+            r_z.append(send(p.at[j], from_z.at[j - 1], "sp", 4 if j == 2 else 2))
+    for copy, slot in ((r_z[1], 0), (r_z[2], 1)):
+        copy.wait_recv()
+        total = total + from_z[slot].astype(jnp.float32)
     channel = total.astype(jnp.bfloat16).astype(jnp.float32)
     updated[...] = (stream[...] + 0.5 * row_norm(channel, after_gain[...], 1e-06)).astype(
         updated.dtype
@@ -371,9 +402,6 @@
     inner, units_all = gate_weight.shape
     units = units_all // depth
     span = down_weight.shape[1]
-    pair = jnp.concatenate([key_pairs, values], axis=1)
-    gate_in = jnp.transpose(gate_weight.reshape(inner, depth, units), (1, 0, 2))
-    up_in = jnp.transpose(up_weight.reshape(inner, depth, units), (1, 0, 2))
     down_in = down_weight.reshape(depth, units, span)
     tiles = 4 * depth
     total_sends = 7 * (depth - 1) + 4 + 3 + 3 * depth - 3 + n_tp - 1 + 2 * tiles
@@ -384,10 +412,13 @@
     return pl.pallas_call(
         layer,
         out_shape=jax.ShapeDtypeStruct(residual.shape, bf16),
-        in_specs=[vmem, vmem, vmem, smem] + [vmem] * 5 + [hbm] * 3,
+        in_specs=[vmem] * 4 + [smem] + [vmem] * 7 + [hbm],
         out_specs=vmem,
         scratch_shapes=[
-            pltpu.VMEM((n_sp,) + pair.shape, bf16),
+            pltpu.VMEM((depth, inner, units), bf16),
+            pltpu.VMEM((depth, inner, units), bf16),
+            pltpu.VMEM((tiles // 2, 2 * quarter, units), bf16),
+            pltpu.VMEM((n_sp, tokens_here, 2 * key_pairs.shape[1]), bf16),
             pltpu.VMEM((n_sp, inner, units), bf16),
             pltpu.VMEM((n_sp, inner, units), bf16),
             pltpu.VMEM((n_sp, units, span), bf16),
@@ -409,15 +440,16 @@
     )(
         residual,
         queries,
-        pair,
+        key_pairs,
+        values,
         lambdas,
         head_gain[None],
         out_weight,
         mixer_gain[None],
         before_gain[None],
         after_gain[None],
-        gate_in,
-        up_in,
+        gate_weight,
+        up_weight,
         down_in,
     )
 

time: 156 us -> 124 us (0.79)
  the two profiles are of different devices: /device:TPU:16 before, /device:TPU:1 now
where the time goes in v2:
time: 124 us
  Pallas kernels  122 us (98%)
  local copies, waits for them, and re-layouts  1.67 us (1%)
    pallas_call x1, Pallas kernels, one_kernel(): pl.pallas_call(layer, out_shape=jax.ShapeDtypeStruct(residual.shape, bf16...  122 us

profile of v2, /device:TPU:1, one launch (start us, length us, event | category | flops | bytes accessed | tf_op | source)
XLA Modules:
  0.0 123.6 jit_solution(6989869318159038939)
XLA Ops:
  0.0 121.9 %shard_map.127 = bf16[64,2048]{1,0:T(8,128)(2,1)} custom-call(bf16[64,2048]{1,0:T(8,128)(2,1)} %residual.1, bf16[256,256]{1,0:T(8,128)(2,1)} %queries.1, bf16[256,128]{1,0:T(8,128)(2,1)} %key_pairs.1, bf16[256,128]{1,0:T(8,128)(2,1)} %values.1, f32[2]{0:T(128)} %lambdas.1, f32[1,128]{1,0:T(1,128)} %bitcast.9, bf16[1024,2048]{1,0:T(8,128)(2,1)} %out_weight.1, ...), custom_call_target="tpu_custom_call" | custom-call | tf_op jit(solution)/shard_map/pallas_call | solution.py:412
  121.9 1.7 %copy.15 = bf16[64,2048]{1,0:T(8,128)(2,1)} copy(bf16[64,2048]{1,0:T(8,128)(2,1)} %shard_map.127) | data formatting | bytes 524288

commit v3 on v2

--- a/solution.py
+++ b/solution.py
@@ -231,6 +231,9 @@
 
     gate_moves = scatter(gate_in, gate_w, 0)
     up_moves = scatter(up_in, up_w, 1)
+    down_local = pltpu.make_async_copy(down_in.at[place // 2], down_w.at[place], local_sems.at[2])
+    down_local.start()
+    down_x = [send(down_in.at[place // 2], down_w.at[place], "sp", 1)]
     for j, copy in ((1, near), (3, relayed)):
         copy.wait_recv()
         kv_x.append(send(kv.at[j], kv.at[depth + j], "sp", 1))
@@ -286,7 +289,10 @@
     up_x = forward(up_w, up_moves[1])
     far.wait_recv()
     relayed = send(x.at[2], x.at[3], "sp", 2)
-    down_moves = scatter(down_in, down_w, 2)
+    down_z = [
+        send(down_in.at[flip(place, 2 * j) // 2], down_w.at[place], "sp", 2 * j)
+        for j in range(1, depth)
+    ]
     order = ((2, far), (1, near), (3, relayed))
     for j, copy in order:
         if j != 2:
@@ -325,10 +331,13 @@
 
     group(0, widen)
     x_last = []
-    for j, copy in zip((0, 2, 1, 3), x_y):
-        copy.wait_recv()
+    for i, j in enumerate((0, 2, 1, 3)):
+        if i:
+            down_z[i - 1].wait_recv()
+            slot = down_w.at[flip(place, 2 * i)]
+            down_x.append(send(slot, slot, "sp", 1))
+        x_y[i].wait_recv()
         x_last.append(send(x.at[depth + j], x.at[half + depth + j], "tp", 1))
-    down_x = forward(down_w, down_moves[1])
     for copy in x_c:
         copy.wait_recv()
     group(2, widen)
@@ -336,8 +345,7 @@
     for copy in x_last:
         copy.wait_recv()
     group(3, widen)
-    down_moves[0].wait()
-    down_moves[2].wait_recv()
+    down_local.wait()
     for copy in down_x:
         copy.wait_recv()
     group(3, narrow)

time: 124 us -> 125 us (level)
    pallas_call x1, Pallas kernels: 122 us -> 123 us  [one_kernel(): pl.pallas_call(layer, out_shape=jax.ShapeDtypeStruct(residual.shape, bf16...]
where the time goes in v3:
time: 125 us
  Pallas kernels  123 us (98%)
  local copies, waits for them, and re-layouts  1.67 us (1%)
    pallas_call x1, Pallas kernels, one_kernel(): pl.pallas_call(layer, out_shape=jax.ShapeDtypeStruct(residual.shape, bf16...  123 us

profile of v3, /device:TPU:1, one launch (start us, length us, event | category | flops | bytes accessed | tf_op | source)
XLA Modules:
  0.0 125.0 jit_solution(16350109536646660201)
XLA Ops:
  0.0 123.3 %shard_map.127 = bf16[64,2048]{1,0:T(8,128)(2,1)} custom-call(bf16[64,2048]{1,0:T(8,128)(2,1)} %residual.1, bf16[256,256]{1,0:T(8,128)(2,1)} %queries.1, bf16[256,128]{1,0:T(8,128)(2,1)} %key_pairs.1, bf16[256,128]{1,0:T(8,128)(2,1)} %values.1, f32[2]{0:T(128)} %lambdas.1, f32[1,128]{1,0:T(1,128)} %bitcast.9, bf16[1024,2048]{1,0:T(8,128)(2,1)} %out_weight.1, ...), custom_call_target="tpu_custom_call" | custom-call | tf_op jit(solution)/shard_map/pallas_call | solution.py:420
  123.3 1.7 %copy.15 = bf16[64,2048]{1,0:T(8,128)(2,1)} copy(bf16[64,2048]{1,0:T(8,128)(2,1)} %shard_map.127) | data formatting | bytes 524288
